TPU v7x, 768 devices: a whole 4x8x12 slice. The times are simulated.
768 devices in a mesh: kv: 192 (over z, y, core), tp: 4 (over x).
Axes of the slice: x: 4, y: 8, z: 12, core: 2. Of those that a mesh axis runs over, the one named last changes fastest.
Arguments:
- queries: bfloat16 [49152, 3072], P('kv', 'tp'), may hold values from -6 to 6
- keys: bfloat16 [49152, 512], P('kv', 'tp'), may hold values from -6 to 6
- values: bfloat16 [49152, 512], P('kv', 'tp'), may hold values from -6 to 6
- log_sums: float32 [24, 49152], P('tp', 'kv'), may hold values from 6 to 7.5
- out_grad: bfloat16 [49152, 3072], P('kv', 'tp'), may hold values from -6 to 6
- chosen: int32 [768, 4, 8], P('kv', 'tp'), may hold values from 0 to 767, as said below
- inputs: bfloat16 [49152, 3072], P('kv', 'tp'), may hold values from -6 to 6
Outputs:
- query_grad: bfloat16 [49152, 3072], P('kv', 'tp')
- key_grad: bfloat16 [49152, 512], P('kv', 'tp')
- value_grad: bfloat16 [49152, 512], P('kv', 'tp')
- weight_grad: float32 [3072, 512], P('kv', 'tp')
Inputs may be any that keep to these rules, and one draw needn't show every extreme that they name: `chosen`: for query block g and key head h, every slot holds g (an empty slot) or a key block c with g - 16 <= c < g; the blocks of the live slots of one list are distinct; each list has between 4 and 8 live slots, except that query block g has at most g of them (block 0 has none).
All inputs are finite; a program needn't handle non-finite values.
Results may differ from a plain program's by a relative error of at most 0.0049.
Values may be sent and summed in bfloat16 or wider, within the bound.
A program may use at most 32 MiB of HBM per device.

v0:
```python
import jax
import jax.numpy as jnp
from jax import lax
from jax.sharding import Mesh
from jax.sharding import PartitionSpec as P

REACH = 4
KV = ("kv_0", "kv_1", "kv_2")


def passed_along(value, axis, steps):
    count = lax.axis_size(axis)
    leading, last = (max(0, -steps), min(count, count - steps))
    return lax.ppermute(value, axis, [(source, source + steps) for source in range(leading, last)])


def sent_to_all(x, axis):
    copies = jnp.broadcast_to(x, (lax.axis_size(axis), *x.shape))
    return lax.all_to_all(copies, axis, split_axis=0, concat_axis=0, tiled=True)


def in_order(pieces, dim):
    pieces = jnp.moveaxis(pieces, 0, dim)
    shape = pieces.shape
    return pieces.reshape(*shape[:dim], shape[dim] * shape[dim + 1], *shape[dim + 2 :])


def gather_directly(x, axis, dim):
    pieces = sent_to_all(x, axis)
    return in_order(pieces, dim)


def own_block(pieces, axes, sequence):
    shape = [lax.axis_size(a) for a in axes]
    pieces = pieces.reshape(*shape, *pieces.shape[1:])
    pieces = pieces.transpose(*sequence, *range(len(axes), pieces.ndim))
    pieces = pieces.reshape(-1, *pieces.shape[len(axes) :])
    for k in sequence:
        pieces = lax.psum_scatter(pieces, axes[k], scatter_dimension=0, tiled=True)
    return pieces[0]


def split_up(x, dim, length):
    before, after = (x.shape[:dim], x.shape[dim + 1 :])
    return jnp.moveaxis(x.reshape(*before, length, -1, *after), dim, 0)


def summed_rows(x, axes, sequence, dim):
    length = lax.axis_size(axes)
    return own_block(split_up(x, dim, length), axes, sequence)


def tile_grads(
    query_tile_set,
    gradient_tiles,
    sum_tiles,
    key_matrix_rows,
    value_matrix_rows,
    permitted_mask,
    scaling,
):
    scores = (
        jnp.einsum(
            "nevu,npu->nvep", query_tile_set, key_matrix_rows, preferred_element_type=jnp.float32
        )
        * scaling
    )
    weights = jnp.where(permitted_mask[:, None], jnp.exp(scores - sum_tiles[..., None]), 0.0)
    grad_weights = jnp.einsum(
        "nevu,npu->nvep", gradient_tiles, value_matrix_rows, preferred_element_type=jnp.float32
    )
    delta_rows = jnp.sum(weights * grad_weights, -1, keepdims=True)
    score_gradient = (weights * (grad_weights - delta_rows)).astype(jnp.bfloat16)
    weights_reduced = weights.astype(jnp.bfloat16)
    query_part = (
        jnp.einsum(
            "nlpv,nvu->nplu", score_gradient, key_matrix_rows, preferred_element_type=jnp.float32
        )
        * scaling
    )
    key_part = (
        jnp.einsum(
            "cxie,cixa->cea", score_gradient, query_tile_set, preferred_element_type=jnp.float32
        )
        * scaling
    )
    value_part = jnp.einsum(
        "cxie,cixa->cea", weights_reduced, gradient_tiles, preferred_element_type=jnp.float32
    )
    return (query_part, key_part, value_part)


def shards(queries, keys, values, log_sums, out_grad, chosen, inputs):
    tok_rows = keys.shape[0]
    blocks_dev = chosen.shape[0]
    block_length = tok_rows // blocks_dev
    head_dim = keys.shape[1]
    group_size = queries.shape[1] // head_dim
    scaling = head_dim ** (-0.5)
    window_blocks = (REACH + 1) * blocks_dev
    device = lax.axis_index(KV)
    earlier = []
    for offset in range(REACH, 0, -1):
        earlier.append(passed_along((keys, values), KV, offset))
    win_keys = jnp.concatenate([pair[0] for pair in earlier] + [keys], 0)
    win_values = jnp.concatenate([pair[1] for pair in earlier] + [values], 0)
    listed = chosen[:, 0, :]
    global_ids = device * blocks_dev + jnp.arange(blocks_dev, dtype=jnp.int32)
    live_slots = listed < global_ids[:, None]
    local_ids = listed - (device - REACH) * blocks_dev
    own_index = REACH * blocks_dev + jnp.arange(blocks_dev, dtype=jnp.int32)
    query_tile_set = queries.reshape(blocks_dev, block_length, group_size, head_dim)
    gradient_tiles = out_grad.reshape(blocks_dev, block_length, group_size, head_dim)
    sum_tiles = log_sums.reshape(group_size, blocks_dev, block_length).transpose(1, 0, 2)
    row_offsets = jnp.arange(block_length, dtype=jnp.int32)
    block_range = jnp.arange(window_blocks, dtype=jnp.int32)
    hits = jnp.any((local_ids[..., None] == block_range) & live_slots[..., None], axis=1)
    own_hit = block_range[None, :] == own_index[:, None]
    key_offsets = jnp.tile(row_offsets, window_blocks)
    causal = key_offsets[None, None, :] <= row_offsets[None, :, None]
    permitted_mask = (
        jnp.repeat(hits, block_length, axis=1)[:, None, :]
        | jnp.repeat(own_hit, block_length, axis=1)[:, None, :] & causal
    )

    def visit(carry, tiles):
        key_acc, value_acc = carry
        query_one, grad_one, sum_one, mask_one = tiles
        query_part, key_part, value_part = tile_grads(
            query_one[None],
            grad_one[None],
            sum_one[None],
            win_keys[None],
            win_values[None],
            mask_one[None],
            scaling,
        )
        return ((key_acc + key_part[0], value_acc + value_part[0]), query_part[0])

    zeros_acc = jnp.zeros((window_blocks * block_length, head_dim), jnp.float32)
    (key_window, value_window), query_blocks = lax.scan(
        visit, (zeros_acc, zeros_acc), (query_tile_set, gradient_tiles, sum_tiles, permitted_mask)
    )
    key_pieces = key_window.reshape(REACH + 1, tok_rows, head_dim)
    value_pieces = value_window.reshape(REACH + 1, tok_rows, head_dim)
    query_grad = query_blocks.reshape(tok_rows, group_size * head_dim).astype(jnp.bfloat16)
    key_total = key_pieces[REACH]
    value_total = value_pieces[REACH]
    for offset in range(1, REACH + 1):
        back_key, back_value = passed_along(
            (key_pieces[REACH - offset], value_pieces[REACH - offset]), KV, -offset
        )
        key_total = key_total + back_key
        value_total = value_total + back_value
    key_grad = key_total.astype(jnp.bfloat16)
    value_grad = value_total.astype(jnp.bfloat16)
    whole_inputs = gather_directly(inputs, "tp", 1)
    weight_grad = summed_rows(
        lax.dot_general(
            whole_inputs, value_grad, (((0,), (0,)), ((), ())), preferred_element_type=jnp.float32
        ),
        KV,
        (2, 0, 1),
        0,
    )
    return (query_grad, key_grad, value_grad, weight_grad)


def solution(mesh):
    split = Mesh(mesh.devices.reshape(12, 8, 2, mesh.shape["tp"]), ("kv_0", "kv_1", "kv_2", "tp"))
    return jax.shard_map(
        shards,
        mesh=split,
        in_specs=(
            P(KV, "tp"),
            P(KV, "tp"),
            P(KV, "tp"),
            P("tp", KV),
            P(KV, "tp"),
            P(KV, "tp", None),
            P(KV, "tp"),
        ),
        out_specs=(P(KV, "tp"), P(KV, "tp"), P(KV, "tp"), P(KV, "tp")),
        check_vma=False,
    )
```

profile of v0, /device:TPU:6, one launch (start us, length us, event | category | flops | bytes accessed | tf_op | source)
XLA Modules:
  0.0 253.3 jit_solution(4639076016614622900)
XLA Ops:
  7.2 4.5 %collective-permute-start = (bf16[256,128]{1,0:T(8,128)(2,1)}, bf16[256,128]{1,0:T(8,128)(2,1)S(1)}, u32[]{:S(2)}, u32[]{:S(2)}) collective-permute-start(bf16[256,128]{1,0:T(8,128)(2,1)} %param.10), channel_id=1, source_target_pairs={{0,16},{4,20},{8,24},{12,28},{16,32},{20,36},{24,40},{28,44},{32,4... | collective-permute-start | bytes 196616 | tf_op jit(solution)/shard_map/ppermute | solution.py:14
  11.7 2.6 %collective-permute-start.1 = (bf16[256,128]{1,0:T(8,128)(2,1)}, bf16[256,128]{1,0:T(8,128)(2,1)S(1)}, u32[]{:S(2)}, u32[]{:S(2)}) collective-permute-start(bf16[256,128]{1,0:T(8,128)(2,1)} %param.10), channel_id=1, source_target_pairs={{0,12},{4,16},{8,20},{12,24},{16,28},{20,32},{24,36},{28,40},{32,4... | collective-permute-start | bytes 196616 | tf_op jit(solution)/shard_map/ppermute | solution.py:14
  14.3 4.7 %collective-permute-start.2 = (bf16[256,128]{1,0:T(8,128)(2,1)}, bf16[256,128]{1,0:T(8,128)(2,1)S(1)}, u32[]{:S(2)}, u32[]{:S(2)}) collective-permute-start(bf16[256,128]{1,0:T(8,128)(2,1)} %param.10), channel_id=1, source_target_pairs={{0,8},{4,12},{8,16},{12,20},{16,24},{20,28},{24,32},{28,36},{32,40... | collective-permute-start | bytes 196616 | tf_op jit(solution)/shard_map/ppermute | solution.py:14
  19.0 2.7 %collective-permute-start.3 = (bf16[256,128]{1,0:T(8,128)(2,1)}, bf16[256,128]{1,0:T(8,128)(2,1)S(1)}, u32[]{:S(2)}, u32[]{:S(2)}) collective-permute-start(bf16[256,128]{1,0:T(8,128)(2,1)} %param.10), channel_id=1, source_target_pairs={{0,4},{4,8},{8,12},{12,16},{16,20},{20,24},{24,28},{28,32},{32,36}... | collective-permute-start | bytes 196616 | tf_op jit(solution)/shard_map/ppermute | solution.py:14
  21.7 2.7 %collective-permute-start.4 = (bf16[256,128]{1,0:T(8,128)(2,1)}, bf16[256,128]{1,0:T(8,128)(2,1)S(1)}, u32[]{:S(2)}, u32[]{:S(2)}) collective-permute-start(bf16[256,128]{1,0:T(8,128)(2,1)} %param.11), channel_id=1, source_target_pairs={{0,16},{4,20},{8,24},{12,28},{16,32},{20,36},{24,40},{28,44},{32,4... | collective-permute-start | bytes 196616 | tf_op jit(solution)/shard_map/ppermute | solution.py:14
  26.9 4.9 %all-to-all-start = ((bf16[4,256,768]{1,2,0:T(8,128)(2,1)}), bf16[4,256,768]{1,2,0:T(8,128)(2,1)}, u32[]{:S(2)}, u32[]{:S(2)}) async-start(bf16[4,256,768]{1,2,0:T(8,128)(2,1)} %broadcast_in_dim.49), calls=%async_computation | async-start | bytes 3145728 | tf_op jit(solution)/shard_map/all_to_all | solution.py:19
  35.5 2.5 %collective-permute-start.5 = (bf16[256,128]{1,0:T(8,128)(2,1)S(1)}, bf16[256,128]{1,0:T(8,128)(2,1)S(1)}, u32[]{:S(2)}, u32[]{:S(2)}) collective-permute-start(bf16[256,128]{1,0:T(8,128)(2,1)S(1)} %copy-done.7), channel_id=1, source_target_pairs={{0,12},{4,16},{8,20},{12,24},{16,28},{20,32},{24,36},{28,40},{32,4... | collective-permute-start | bytes 196616 | tf_op jit(solution)/shard_map/ppermute | solution.py:14
  38.1 3.5 %collective-permute-start.6 = (bf16[256,128]{1,0:T(8,128)(2,1)S(1)}, bf16[256,128]{1,0:T(8,128)(2,1)S(1)}, u32[]{:S(2)}, u32[]{:S(2)}) collective-permute-start(bf16[256,128]{1,0:T(8,128)(2,1)S(1)} %copy-done.7), channel_id=1, source_target_pairs={{0,8},{4,12},{8,16},{12,20},{16,24},{20,28},{24,32},{28,36},{32,40... | collective-permute-start | bytes 196616 | tf_op jit(solution)/shard_map/ppermute | solution.py:14
  41.6 3.7 %collective-permute-start.7 = (bf16[256,128]{1,0:T(8,128)(2,1)S(1)}, bf16[256,128]{1,0:T(8,128)(2,1)S(1)}, u32[]{:S(2)}, u32[]{:S(2)}) collective-permute-start(bf16[256,128]{1,0:T(8,128)(2,1)S(1)} %copy-done.7), channel_id=1, source_target_pairs={{0,4},{4,8},{8,12},{12,16},{16,20},{20,24},{24,28},{28,32},{32,36}... | collective-permute-start | bytes 196616 | tf_op jit(solution)/shard_map/ppermute | solution.py:14
  48.6 38.2 %while.15 = (s32[]{:T(128)}, f32[1280,128]{1,0:T(8,128)}, f32[1280,128]{1,0:T(8,128)}, bf16[4,64,6,128]{3,1,2,0:T(8,128)(2,1)}, pred[4,64,1280]{2,1,0:T(8,128)(4...) while((s32[]{:T(128)}, f32[1280,128]{1,0:T(8,128)}, ...), condition=%wide.region_3.4_spmd.clone, body=%wide.region_1.3_spmd.clone.sunk | while | flops 634437248 | bytes 22346948 | solution.py:141
  48.6 1.6 convolution_bitcast_fusion.5
  52.2 2.2 fusion.56
  55.5 2.3 fusion.57
  57.8 1.6 convolution_bitcast_fusion.5
  61.4 2.5 fusion.56
  64.9 2.5 fusion.57
  67.4 1.6 convolution_bitcast_fusion.5
  71.1 2.5 fusion.56
  74.6 2.5 fusion.57
  77.1 1.6 convolution_bitcast_fusion.5
  80.8 2.5 fusion.56
  84.3 2.5 fusion.57
  88.0 1.3 collective-permute-start.12
  89.3 1.3 collective-permute-start.13
  93.2 4.6 %collective-permute-done.13 = f32[256,128]{1,0:T(8,128)S(1)} collective-permute-done((f32[256,128]{1,0:T(8,128)S(1)}, f32[256,128]{1,0:T(8,128)S(1)}, u32[]{:S(2)}, u32[]{:S(2)}) %collective-permute-start.13) | collective-permute-done | bytes 131104 | tf_op jit(solution)/shard_map/ppermute | solution.py:14
  97.8 1.3 collective-permute-done.14
  99.1 11.7 %collective-permute-done.15 = f32[256,128]{1,0:T(8,128)S(1)} collective-permute-done((f32[256,128]{1,0:T(8,128)S(1)}, f32[256,128]{1,0:T(8,128)S(1)}, u32[]{:S(2)}, u32[]{:S(2)}) %collective-permute-start.15) | collective-permute-done | bytes 131104 | tf_op jit(solution)/shard_map/ppermute | solution.py:14
  111.7 2.1 convolution_bitcast_fusion.3
  114.3 1.4 copy.32
  115.8 24.5 %reduce-scatter.4.cloned.1.call-done = f32[96,16,128]{2,1,0:T(8,128)} async-done(((f32[192,16,128]{2,1,0:T(8,128)}), f32[96,16,128]{2,1,0:T(8,128)}) %reduce-scatter.4.cloned.1.call-update) | async-done | bytes 786448 | tf_op jit(solution)/shard_map/reduce_scatter | solution.py:39
  147.7 55.4 %reduce-scatter.6.cloned.1.call-done = f32[8,16,128]{2,1,0:T(8,128)} async-done(((f32[96,16,128]{2,1,0:T(8,128)}), f32[8,16,128]{2,1,0:T(8,128)}) %reduce-scatter.6.cloned.1.call-update) | async-done | bytes 65552 | tf_op jit(solution)/shard_map/reduce_scatter | solution.py:39
  203.8 43.0 %reduce-scatter.8.cloned.1.call-done = f32[1,16,128]{2,1,0:T(8,128)} async-done(((f32[8,16,128]{2,1,0:T(8,128)}), f32[1,16,128]{2,1,0:T(8,128)}) %reduce-scatter.8.cloned.1.call-update) | async-done | bytes 8208 | tf_op jit(solution)/shard_map/reduce_scatter | solution.py:39
  (123 shorter events, 34.9 us)
Async XLA Ops:
  7.2 28.3 %collective-permute-start = (bf16[256,128]{1,0:T(8,128)(2,1)}, bf16[256,128]{1,0:T(8,128)(2,1)S(1)}, u32[]{:S(2)}, u32[]{:S(2)}) collective-permute-start(bf16[256,128]{1,0:T(8,128)(2,1)} %param.10), channel_id=1, source_target_pairs={{0,16},{4,20},{8,24},{12,28},{16,32},{20,36},{24,40},{28,44},{32,4... | collective-permute-start | bytes 196616 | tf_op jit(solution)/shard_map/ppermute | solution.py:14
  11.7 26.4 %collective-permute-start.1 = (bf16[256,128]{1,0:T(8,128)(2,1)}, bf16[256,128]{1,0:T(8,128)(2,1)S(1)}, u32[]{:S(2)}, u32[]{:S(2)}) collective-permute-start(bf16[256,128]{1,0:T(8,128)(2,1)} %param.10), channel_id=1, source_target_pairs={{0,12},{4,16},{8,20},{12,24},{16,28},{20,32},{24,36},{28,40},{32,4... | collective-permute-start | bytes 196616 | tf_op jit(solution)/shard_map/ppermute | solution.py:14
  14.3 27.3 %collective-permute-start.2 = (bf16[256,128]{1,0:T(8,128)(2,1)}, bf16[256,128]{1,0:T(8,128)(2,1)S(1)}, u32[]{:S(2)}, u32[]{:S(2)}) collective-permute-start(bf16[256,128]{1,0:T(8,128)(2,1)} %param.10), channel_id=1, source_target_pairs={{0,8},{4,12},{8,16},{12,20},{16,24},{20,28},{24,32},{28,36},{32,40... | collective-permute-start | bytes 196616 | tf_op jit(solution)/shard_map/ppermute | solution.py:14
  19.0 26.3 %collective-permute-start.3 = (bf16[256,128]{1,0:T(8,128)(2,1)}, bf16[256,128]{1,0:T(8,128)(2,1)S(1)}, u32[]{:S(2)}, u32[]{:S(2)}) collective-permute-start(bf16[256,128]{1,0:T(8,128)(2,1)} %param.10), channel_id=1, source_target_pairs={{0,4},{4,8},{8,12},{12,16},{16,20},{20,24},{24,28},{28,32},{32,36}... | collective-permute-start | bytes 196616 | tf_op jit(solution)/shard_map/ppermute | solution.py:14
  21.7 23.7 %collective-permute-start.4 = (bf16[256,128]{1,0:T(8,128)(2,1)}, bf16[256,128]{1,0:T(8,128)(2,1)S(1)}, u32[]{:S(2)}, u32[]{:S(2)}) collective-permute-start(bf16[256,128]{1,0:T(8,128)(2,1)} %param.11), channel_id=1, source_target_pairs={{0,16},{4,20},{8,24},{12,28},{16,32},{20,36},{24,40},{28,44},{32,4... | collective-permute-start | bytes 196616 | tf_op jit(solution)/shard_map/ppermute | solution.py:14
  26.9 5.0 %copy-start.9 = (s32[4,1,8]{2,1,0:T(1,128)S(1)}, s32[4,1,8]{2,1,0:T(1,128)}, u32[]{:S(2)}) copy-start(s32[4,1,8]{2,1,0:T(1,128)} %param.14) | copy-start | bytes 388
  26.9 6.7 %copy-start.3 = (bf16[256,768]{1,0:T(8,128)(2,1)S(1)}, bf16[256,768]{1,0:T(8,128)(2,1)}, u32[]{:S(2)}) copy-start(bf16[256,768]{1,0:T(8,128)(2,1)} %param.9) | copy-start | bytes 1179652
  26.9 84.9 %all-to-all-start = ((bf16[4,256,768]{1,2,0:T(8,128)(2,1)}), bf16[4,256,768]{1,2,0:T(8,128)(2,1)}, u32[]{:S(2)}, u32[]{:S(2)}) async-start(bf16[4,256,768]{1,2,0:T(8,128)(2,1)} %broadcast_in_dim.49), calls=%async_computation | async-start | bytes 3145728 | tf_op jit(solution)/shard_map/all_to_all | solution.py:19
  31.8 108.5 %reduce-scatter.4.cloned.1.call-start = ((), (), s32[]{:S(2)}) async-start(), calls=%async_computation.4 | async-start | bytes 2359296 | tf_op jit(solution)/shard_map/reduce_scatter | solution.py:39
  32.6 2.9 %copy-start.8 = (f32[6,256]{1,0:T(8,128)S(1)}, f32[6,256]{1,0:T(8,128)}, u32[]{:S(2)}) copy-start(f32[6,256]{1,0:T(8,128)} %param.12) | copy-start | bytes 18436
  32.6 2.9 %copy-start.7 = (bf16[256,128]{1,0:T(8,128)(2,1)S(1)}, bf16[256,128]{1,0:T(8,128)(2,1)}, u32[]{:S(2)}) copy-start(bf16[256,128]{1,0:T(8,128)(2,1)} %param.11) | copy-start | bytes 196612
  33.5 11.8 %copy-start.6 = (bf16[256,128]{1,0:T(8,128)(2,1)S(1)}, bf16[256,128]{1,0:T(8,128)(2,1)}, u32[]{:S(2)}) copy-start(bf16[256,128]{1,0:T(8,128)(2,1)} %param.10) | copy-start | bytes 196612
  35.5 10.5 %collective-permute-start.5 = (bf16[256,128]{1,0:T(8,128)(2,1)S(1)}, bf16[256,128]{1,0:T(8,128)(2,1)S(1)}, u32[]{:S(2)}, u32[]{:S(2)}) collective-permute-start(bf16[256,128]{1,0:T(8,128)(2,1)S(1)} %copy-done.7), channel_id=1, source_target_pairs={{0,12},{4,16},{8,20},{12,24},{16,28},{20,32},{24,36},{28,40},{32,4... | collective-permute-start | bytes 196616 | tf_op jit(solution)/shard_map/ppermute | solution.py:14
  38.1 8.6 %collective-permute-start.6 = (bf16[256,128]{1,0:T(8,128)(2,1)S(1)}, bf16[256,128]{1,0:T(8,128)(2,1)S(1)}, u32[]{:S(2)}, u32[]{:S(2)}) collective-permute-start(bf16[256,128]{1,0:T(8,128)(2,1)S(1)} %copy-done.7), channel_id=1, source_target_pairs={{0,8},{4,12},{8,16},{12,20},{16,24},{20,28},{24,32},{28,36},{32,40... | collective-permute-start | bytes 196616 | tf_op jit(solution)/shard_map/ppermute | solution.py:14
  41.6 5.7 %collective-permute-start.7 = (bf16[256,128]{1,0:T(8,128)(2,1)S(1)}, bf16[256,128]{1,0:T(8,128)(2,1)S(1)}, u32[]{:S(2)}, u32[]{:S(2)}) collective-permute-start(bf16[256,128]{1,0:T(8,128)(2,1)S(1)} %copy-done.7), channel_id=1, source_target_pairs={{0,4},{4,8},{8,12},{12,16},{16,20},{20,24},{24,28},{28,32},{32,36}... | collective-permute-start | bytes 196616 | tf_op jit(solution)/shard_map/ppermute | solution.py:14
  48.6 3.3 %copy-start.1 = (bf16[4,64,6,128]{3,1,2,0:T(8,128)(2,1)}, bf16[4,64,6,128]{3,1,2,0:T(8,128)(2,1)S(1)}, u32[]{:S(2)}) copy-start(bf16[4,64,6,128]{3,1,2,0:T(8,128)(2,1)S(1)} %get-tuple-element.248) | copy-start | bytes 1179652 | tf_op jit(solution)/shard_map/while
  57.8 3.3 %copy-start.1 = (bf16[4,64,6,128]{3,1,2,0:T(8,128)(2,1)}, bf16[4,64,6,128]{3,1,2,0:T(8,128)(2,1)S(1)}, u32[]{:S(2)}) copy-start(bf16[4,64,6,128]{3,1,2,0:T(8,128)(2,1)S(1)} %get-tuple-element.248) | copy-start | bytes 1179652 | tf_op jit(solution)/shard_map/while
  64.9 2.5 copy-start.2
  67.4 3.4 %copy-start.1 = (bf16[4,64,6,128]{3,1,2,0:T(8,128)(2,1)}, bf16[4,64,6,128]{3,1,2,0:T(8,128)(2,1)S(1)}, u32[]{:S(2)}) copy-start(bf16[4,64,6,128]{3,1,2,0:T(8,128)(2,1)S(1)} %get-tuple-element.248) | copy-start | bytes 1179652 | tf_op jit(solution)/shard_map/while
  77.1 3.4 %copy-start.1 = (bf16[4,64,6,128]{3,1,2,0:T(8,128)(2,1)}, bf16[4,64,6,128]{3,1,2,0:T(8,128)(2,1)S(1)}, u32[]{:S(2)}) copy-start(bf16[4,64,6,128]{3,1,2,0:T(8,128)(2,1)S(1)} %get-tuple-element.248) | copy-start | bytes 1179652 | tf_op jit(solution)/shard_map/while
  88.0 5.2 %collective-permute-start.12 = (f32[256,128]{1,0:T(8,128)S(1)}, f32[256,128]{1,0:T(8,128)S(1)}, u32[]{:S(2)}, u32[]{:S(2)}) collective-permute-start(f32[256,128]{1,0:T(8,128)S(1)} %get-tuple-element.146), channel_id=1, source_target_pairs={{4,0},{8,4},{12,8},{16,12},{20,16},{24,20},{28,24},{32,28},{36,32}... | collective-permute-start | bytes 393224 | tf_op jit(solution)/shard_map/ppermute | solution.py:14
  89.3 8.5 %collective-permute-start.13 = (f32[256,128]{1,0:T(8,128)S(1)}, f32[256,128]{1,0:T(8,128)S(1)}, u32[]{:S(2)}, u32[]{:S(2)}) collective-permute-start(f32[256,128]{1,0:T(8,128)S(1)} %get-tuple-element.147), channel_id=1, source_target_pairs={{8,0},{12,4},{16,8},{20,12},{24,16},{28,20},{32,24},{36,28},{40,32... | collective-permute-start | bytes 393224 | tf_op jit(solution)/shard_map/ppermute | solution.py:14
  90.6 8.5 %collective-permute-start.14 = (f32[256,128]{1,0:T(8,128)S(1)}, f32[256,128]{1,0:T(8,128)S(1)}, u32[]{:S(2)}, u32[]{:S(2)}) collective-permute-start(f32[256,128]{1,0:T(8,128)S(1)} %get-tuple-element.149), channel_id=1, source_target_pairs={{12,0},{16,4},{20,8},{24,12},{28,16},{32,20},{36,24},{40,28},{44,3... | collective-permute-start | bytes 393224 | tf_op jit(solution)/shard_map/ppermute | solution.py:14
  91.9 18.9 %collective-permute-start.15 = (f32[256,128]{1,0:T(8,128)S(1)}, f32[256,128]{1,0:T(8,128)S(1)}, u32[]{:S(2)}, u32[]{:S(2)}) collective-permute-start(f32[256,128]{1,0:T(8,128)S(1)} %get-tuple-element.148), channel_id=1, source_target_pairs={{16,0},{20,4},{24,8},{28,12},{32,16},{36,20},{40,24},{44,28},{48,3... | collective-permute-start | bytes 393224 | tf_op jit(solution)/shard_map/ppermute | solution.py:14
  111.7 2.6 %copy-start.5 = (bf16[256,128]{1,0:T(8,128)(2,1)}, bf16[256,128]{1,0:T(8,128)(2,1)S(1)}, u32[]{:S(2)}) copy-start(bf16[256,128]{1,0:T(8,128)(2,1)S(1)} %add_convert_fusion) | copy-start | bytes 196612
  115.7 24.7 %copy-start = (f32[1280,128]{1,0:T(8,128)S(1)}, f32[1280,128]{1,0:T(8,128)}, u32[]{:S(2)}) copy-start(f32[1280,128]{1,0:T(8,128)} %get-tuple-element.59) | copy-start | bytes 1966084
  115.7 87.4 %reduce-scatter.6.cloned.1.call-start = ((), (), s32[]{:S(2)}) async-start(), calls=%async_computation.5 | async-start | bytes 851968 | tf_op jit(solution)/shard_map/reduce_scatter | solution.py:39
  140.3 106.5 %reduce-scatter.8.cloned.1.call-start = ((), (), s32[]{:S(2)}) async-start(), calls=%async_computation.6 | async-start | bytes 73728 | tf_op jit(solution)/shard_map/reduce_scatter | solution.py:39
  140.4 62.7 %collective-permute-start.10 = (f32[256,128]{1,0:T(8,128)S(1)}, f32[256,128]{1,0:T(8,128)S(1)}, u32[]{:S(2)}, u32[]{:S(2)}) collective-permute-start(f32[256,128]{1,0:T(8,128)S(1)} %get-tuple-element.153), channel_id=1, source_target_pairs={{12,0},{16,4},{20,8},{24,12},{28,16},{32,20},{36,24},{40,28},{44,3... | collective-permute-start | bytes 393224 | tf_op jit(solution)/shard_map/ppermute | solution.py:14
  141.7 61.4 %collective-permute-start.11 = (f32[256,128]{1,0:T(8,128)S(1)}, f32[256,128]{1,0:T(8,128)S(1)}, u32[]{:S(2)}, u32[]{:S(2)}) collective-permute-start(f32[256,128]{1,0:T(8,128)S(1)} %get-tuple-element.152), channel_id=1, source_target_pairs={{16,0},{20,4},{24,8},{28,12},{32,16},{36,20},{40,24},{44,28},{48,3... | collective-permute-start | bytes 393224 | tf_op jit(solution)/shard_map/ppermute | solution.py:14
  143.0 60.2 %collective-permute-start.8 = (f32[256,128]{1,0:T(8,128)S(1)}, f32[256,128]{1,0:T(8,128)S(1)}, u32[]{:S(2)}, u32[]{:S(2)}) collective-permute-start(f32[256,128]{1,0:T(8,128)S(1)} %get-tuple-element.150), channel_id=1, source_target_pairs={{4,0},{8,4},{12,8},{16,12},{20,16},{24,20},{28,24},{32,28},{36,32}... | collective-permute-start | bytes 393224 | tf_op jit(solution)/shard_map/ppermute | solution.py:14
  144.3 58.9 %collective-permute-start.9 = (f32[256,128]{1,0:T(8,128)S(1)}, f32[256,128]{1,0:T(8,128)S(1)}, u32[]{:S(2)}, u32[]{:S(2)}) collective-permute-start(f32[256,128]{1,0:T(8,128)S(1)} %get-tuple-element.151), channel_id=1, source_target_pairs={{8,0},{12,4},{16,8},{20,12},{24,16},{28,20},{32,24},{36,28},{40,32... | collective-permute-start | bytes 393224 | tf_op jit(solution)/shard_map/ppermute | solution.py:14
  (4 other events, 9.6 us)
Sparse Core Ops, SparseCore 0:
  115.8 24.3 reduce-scatter.3
  143.4 59.6 reduce-scatter.5
  206.7 40.0 reduce-scatter.7
where the time goes:
time: 255 us; the launch traced here: 253 us
  waiting for transfers between devices  141 us (55%)
  starting transfers between devices  42.3 us (17%)
  matrix products  35.5 us (14%)
  local copies, waits for them, and re-layouts  16.8 us (7%)
  between operations  14.2 us (6%)
  other arithmetic  3.91 us (2%)
    reduce_scatter x3, waiting for transfers between devices, own_block(): pieces = lax.psum_scatter(pieces, axes[k], scatter_dimension=0, tiled=True)  123 us
    ppermute x16, starting transfers between devices, passed_along(): lax.ppermute(value, axis, [(source, source + steps) for source in range(l...  37.3 us
    ppermute x16, waiting for transfers between devices, passed_along(): lax.ppermute(value, axis, [(source, source + steps) for source in range(l...  17.6 us
    dot_general x4, matrix products, tile_grads(): jnp.einsum('cxie,cixa->cea', weights_reduced, gradient_tiles, preferred_e...  9.81 us
    dot_general x4, matrix products, tile_grads(): jnp.einsum('cxie,cixa->cea', score_gradient, query_tile_set, preferred_el...  9.63 us
    dot_general x4, matrix products, tile_grads(): jnp.einsum('nevu,npu->nvep', gradient_tiles, value_matrix_rows, preferred...  6.29 us
    unnamed x28, local copies, waits for them, and re-layouts  5.54 us
  transfers between devices with their start and end apart: 20, of which 6 were waited for; matrix products, arithmetic and copies ran while one was open for 21% of the time, Pallas kernels for 0%

commit v1 on v0

v1 whole, which is shorter than its diff:
```python
import functools

import jax
import jax.numpy as jnp
from jax import lax
from jax.experimental import pallas as pl
from jax.experimental.pallas import tpu as pltpu
from jax.sharding import PartitionSpec as P

MESH = pl.DeviceIdType.MESH
LOG2E = 1.4426950408889634
MASKED = -1e30

NX, NY, NZ = 4, 8, 12
NCHIP = NY * NZ
T = 256
HD = 128
G = 6
BL = 64
NB = 4
SELS = 8
CPX = NCHIP // NX
RW = 16
HR = CPX * RW

NN = (((1,), (0,)), ((), ()))
NT = (((1,), (1,)), ((), ()))
TN = (((0,), (0,)), ((), ()))


def mm(a, b, dims):
    return lax.dot_general(a, b, dims, preferred_element_type=jnp.float32)


def kernel(
    q_hbm, k_hbm, v_hbm, lse_hbm, do_hbm, ch_ref, in_hbm,
    dq_hbm, dk_hbm, dv_hbm, dw_hbm,
    q6, do6, in6, lse, kbuf, vbuf, hitb, ownb, pst, dpst, dvacc, dkacc, dqst,
    hs, ing, sxv, rxv, sretv, rretv, sxk, rxk, sretk, rretk, vg, kg,
    wpart, r1z, r1y, s1z, s1y, r2z, r2y, dwst,
    lsem, ssem, k_rs, v_rs, in_rs, x_rs, ret_rs, vg_rs, z_rs, y_rs, zs_s, ys_s, osem,
):
    kv = lax.axis_index("kv")
    x = lax.axis_index("tp")
    p = kv // 2
    c = kv % 2
    z = p // NY
    y = p % NY
    o = 1 - c

    def chip(step):
        return lax.rem(p + step + NCHIP, NCHIP)

    def at(chip_id, core):
        return (chip_id * 2 + core, x)

    partner = at(p, o)
    nxt, nxt2, prv, prv2 = (at(chip(s), c) for s in (1, 2, -1, -2))
    xr, xl = lax.rem(x + 1, NX), lax.rem(x + NX - 1, NX)

    barrier = pltpu.get_barrier_semaphore()
    peers = [partner, nxt, nxt2, prv, prv2]
    peers += [(p * 2 + d, xx) for xx in (xr, xl) for d in (0, 1)]
    for d in range(1, NZ):
        peers.append(at(lax.rem(z + d, NZ) * NY + y, c))
    for d in range(1, NY):
        peers.append(at(z * NY + lax.rem(y + d, NY), c))
    for peer in peers:
        pl.semaphore_signal(barrier, inc=1, device_id=peer, device_id_type=MESH)

    loads = []

    def load(src, dst, n):
        copy = pltpu.make_async_copy(src, dst, lsem.at[n])
        copy.start()
        return copy

    ld_k = load(k_hbm, kbuf.at[4 + c], 0)
    ld_q = [load(q_hbm.at[:, pl.ds(HD * h, HD)], q6.at[h], 1 + h) for h in range(G)]
    ld_l = load(lse_hbm, lse, 7)
    ld_v = load(v_hbm, vbuf.at[4 + c], 8)
    ld_i = [load(in_hbm.at[:, pl.ds(HD * h, HD)], in6.at[h], 9 + h) for h in range(G)]
    ld_d = [load(do_hbm.at[:, pl.ds(HD * h, HD)], do6.at[h], 15 + h) for h in range(G)]

    base = (p - 2) * 4 * 2 + 4 * c
    own0 = kv * NB
    wid = lax.broadcasted_iota(jnp.int32, (24, T), 0)
    lane = lax.broadcasted_iota(jnp.int32, (24, T), 1)
    hit = jnp.zeros((24, T), jnp.float32)
    for b in range(NB):
        in_b = (lane // BL) == b
        for k in range(SELS):
            named = ch_ref[b, 0, k]
            slot = jnp.where(named < own0 + b, named - base, -1)
            hit = jnp.where(in_b & (wid == slot), 1.0, hit)
    hitb[...] = jnp.where(hit > 0.5, 0.0, MASKED)
    krow = lax.broadcasted_iota(jnp.int32, (BL, T), 0)
    qlane = lax.broadcasted_iota(jnp.int32, (BL, T), 1)
    for j in range(NB):
        here = (qlane // BL) == j
        causal = here & (krow <= qlane - BL * j)
        ownb[j] = jnp.where(causal, 0.0, jnp.where(here, MASKED, hitb[16 + j : 17 + j, :]))

    for j in range(G):
        ld_i[j].wait()
        xt = in6[j].T
        for m in range(4):
            for d in range(2):
                r0 = (4 * j + m) * RW
                hs[d, r0 : r0 + RW, :] = xt[32 * m + 16 * d : 32 * m + 16 * d + 16, :]

    ld_k.wait()
    ld_v.wait()

    sends = []

    def send(src, dst, recv, device):
        n = len(sends)
        copy = pltpu.make_async_remote_copy(
            src_ref=src, dst_ref=dst, send_sem=ssem.at[n], recv_sem=recv,
            device_id=device, device_id_type=MESH,
        )
        copy.start()
        sends.append(copy)
        return copy

    def arrived(dst, recv):
        pltpu.make_async_copy(dst, dst, recv).wait()

    pl.semaphore_wait(barrier, len(peers))

    def kv_send(buf, rs, slot, device):
        send(buf.at[slot], buf.at[slot], rs.at[slot], device)

    def kv_send_to(buf, rs, src_slot, dst_slot, device):
        send(buf.at[src_slot], buf.at[dst_slot], rs.at[dst_slot], device)

    kv_send_to(kbuf, k_rs, 4 + c, 2 + c, nxt)
    kv_send(kbuf, k_rs, 4 + c, partner)
    kv_send_to(vbuf, v_rs, 4 + c, 2 + c, nxt)
    kv_send(vbuf, v_rs, 4 + c, partner)
    send(hs.at[o], ing.at[0, c], in_rs.at[0, c], partner)
    for d in (0, 1):
        send(hs.at[d], ing.at[3, c], in_rs.at[3, c], (p * 2 + d, xr))
        send(hs.at[d], ing.at[1, c], in_rs.at[1, c], (p * 2 + d, xl))

    for copy in ld_q:
        copy.wait()
    ld_l.wait()
    for copy in ld_d:
        copy.wait()

    lse[...] = lse[...] * LOG2E
    factor = HD ** (-0.5) * LOG2E

    def value_terms(s):
        dvacc[s] = jnp.zeros((T, HD), jnp.float32)

        @pl.loop(0, G)
        def _(h):
            scores = mm(kbuf[s + c], q6[h], NT)
            row = lse[pl.ds(h, 1), :]
            for j in range(NB):
                part = scores[BL * j : BL * j + BL, :] * factor
                if s == 4:
                    shift = ownb[j] - row
                else:
                    shift = hitb[4 * s + j : 4 * s + j + 1, :] - row
                pst[s, h, BL * j : BL * j + BL, :] = jnp.exp2(part + shift)
            dvacc[s] += mm(pst[s, h].astype(jnp.bfloat16), do6[h], NN)

    value_terms(4)
    arrived(kbuf.at[2 + c], k_rs.at[2 + c])
    kv_send(kbuf, k_rs, 2 + c, partner)
    kv_send_to(kbuf, k_rs, 2 + c, c, nxt)
    value_terms(2)
    arrived(vbuf.at[2 + c], v_rs.at[2 + c])
    kv_send(vbuf, v_rs, 2 + c, partner)
    kv_send_to(vbuf, v_rs, 2 + c, c, nxt)
    arrived(kbuf.at[2 + o], k_rs.at[2 + o])
    arrived(kbuf.at[4 + o], k_rs.at[4 + o])
    value_terms(3)
    arrived(kbuf.at[c], k_rs.at[c])
    kv_send(kbuf, k_rs, c, partner)
    value_terms(0)
    arrived(kbuf.at[o], k_rs.at[o])
    value_terms(1)

    sxv[0] = dvacc[1].astype(jnp.bfloat16)
    sxv[1] = dvacc[3].astype(jnp.bfloat16)
    send(sxv, rxv, x_rs.at[0], partner)

    for d in (0, 1):
        arrived(ing.at[3, d], in_rs.at[3, d])
        arrived(ing.at[1, d], in_rs.at[1, d])
    send(ing.at[3, 0], ing.at[2, 0], in_rs.at[2, 0], (kv, xr))
    send(ing.at[1, 1], ing.at[2, 1], in_rs.at[2, 1], (kv, xl))
    arrived(vbuf.at[c], v_rs.at[c])
    kv_send(vbuf, v_rs, c, partner)

    arrived(rxv, x_rs.at[0])
    for k in range(2):
        dvacc[2 * k + 2 * o] += rxv[k].astype(jnp.float32)
    sretv[0] = dvacc[0].astype(jnp.bfloat16)
    sretv[1] = dvacc[2].astype(jnp.bfloat16)
    send(sretv.at[0], rretv.at[0], ret_rs.at[0], prv2)
    send(sretv.at[1], rretv.at[1], ret_rs.at[1], prv)

    for slot in (2 + o, 4 + o, o):
        arrived(vbuf.at[slot], v_rs.at[slot])
    for s in range(5):
        dkacc[s] = jnp.zeros((T, HD), jnp.float32)

    def score_terms(first, last):
        @pl.loop(first, last)
        def _(h):
            delta = jnp.zeros((1, T), jnp.float32)
            for s in range(5):
                dp = mm(vbuf[s + c], do6[h], NT)
                dpst[s] = dp
                delta = delta + jnp.sum(pst[s, h] * dp, axis=0, keepdims=True)
            dqt = jnp.zeros((HD, T), jnp.float32)
            for s in range(5):
                ds = (pst[s, h] * (dpst[s] - delta)).astype(jnp.bfloat16)
                dkacc[s] += mm(ds, q6[h], NN)
                dqt = dqt + mm(kbuf[s + c], ds, TN)
            dqst[h] = (dqt * HD ** (-0.5)).T.astype(jnp.bfloat16)

    score_terms(0, G)

    sxk[0] = dkacc[1].astype(jnp.bfloat16)
    sxk[1] = dkacc[3].astype(jnp.bfloat16)
    send(sxk, rxk, x_rs.at[1], partner)

    for k in range(2):
        arrived(rretv.at[k], ret_rs.at[k])
    total = dvacc[4] + rretv[0].astype(jnp.float32) + rretv[1].astype(jnp.float32)
    vg[c] = total.astype(jnp.bfloat16)
    send(vg.at[c], vg.at[c], vg_rs, partner)

    outs = []

    def store(src, dst):
        copy = pltpu.make_async_copy(src, dst, osem.at[len(outs)])
        copy.start()
        outs.append(copy)

    store(vg.at[c], dv_hbm)
    for h in range(G):
        store(dqst.at[h], dq_hbm.at[:, pl.ds(HD * h, HD)])

    arrived(ing.at[0, o], in_rs.at[0, o])
    for d in (0, 1):
        arrived(ing.at[2, d], in_rs.at[2, d])
    arrived(vg.at[o], vg_rs)

    for rel in range(4):
        if rel == 0:
            rows = mm(hs[c], vg[c], NN) + mm(ing[0, o], vg[o], NN)
        else:
            rows = mm(ing[rel, 0], vg[0], NN) + mm(ing[rel, 1], vg[1], NN)
        first = lax.rem(x + rel, NX) * CPX
        if rel == 0:
            first = x * CPX
        tiles = rows.astype(jnp.bfloat16).reshape(CPX, RW, HD)
        for a in range(CPX // NY):
            wpart[lax.div(first, NY) + a] = tiles[a * NY : (a + 1) * NY]

    def fan(n, src, dst, recv, sem, device, start=True):
        copies = []
        for d in range(1, n):
            copy = pltpu.make_async_remote_copy(
                src_ref=src(d), dst_ref=dst.at[d], send_sem=sem.at[d], recv_sem=recv.at[d],
                device_id=device(d), device_id_type=MESH,
            )
            if start:
                copy.start()
            copies.append(copy)
        return copies

    def total_of(n, own, got, recv):
        acc = own.astype(jnp.float32)
        for d in range(1, n):
            arrived(got.at[d], recv.at[d])
            acc = acc + got[d].astype(jnp.float32)
        return acc

    def z_at(d):
        return lax.rem(z + d, NZ)

    def y_at(d):
        return lax.rem(y + d, NY)

    def z_dev(d):
        return at(z_at(d) * NY + y, c)

    def y_dev(d):
        return at(z * NY + y_at(d), c)

    def first_z(start):
        return fan(NZ, lambda d: wpart.at[z_at(d)], r1z, z_rs, zs_s, z_dev, start)

    def first_y(start):
        return fan(NY, lambda d: wpart.at[:, y_at(d)], r1y, y_rs, ys_s, y_dev, start)

    @pl.when(c == 0)
    def _():
        first_z(True)

    @pl.when(c == 1)
    def _():
        first_y(True)

    arrived(rxk, x_rs.at[1])
    for k in range(2):
        dkacc[2 * k + 2 * o] += rxk[k].astype(jnp.float32)
    sretk[0] = dkacc[0].astype(jnp.bfloat16)
    sretk[1] = dkacc[2].astype(jnp.bfloat16)
    send(sretk.at[0], rretk.at[0], ret_rs.at[2], prv2)
    send(sretk.at[1], rretk.at[1], ret_rs.at[3], prv)

    @pl.when(c == 0)
    def _():
        acc = total_of(NZ, wpart[z], r1z, z_rs)
        s1z[...] = acc.astype(jnp.bfloat16)
        second = fan(NY, lambda d: s1z.at[y_at(d)], r2y, y_rs, ys_s, y_dev)
        dwst[...] = total_of(NY, s1z[y], r2y, y_rs)
        for copy in first_z(False) + second:
            copy.wait_send()

    @pl.when(c == 1)
    def _():
        acc = total_of(NY, wpart[:, y], r1y, y_rs)
        s1y[...] = acc.astype(jnp.bfloat16)
        second = fan(NZ, lambda d: s1y.at[z_at(d)], r2z, z_rs, zs_s, z_dev)
        dwst[...] = total_of(NZ, s1y[z], r2z, z_rs)
        for copy in first_y(False) + second:
            copy.wait_send()

    store(dwst, dw_hbm)
    for k in range(2):
        arrived(rretk.at[k], ret_rs.at[2 + k])
    key_total = dkacc[4] + rretk[0].astype(jnp.float32) + rretk[1].astype(jnp.float32)
    kg[...] = (key_total * HD ** (-0.5)).astype(jnp.bfloat16)
    store(kg, dk_hbm)
    for copy in sends:
        copy.wait_send()
    for copy in outs:
        copy.wait()


def shards(queries, keys, values, log_sums, out_grad, chosen, inputs):
    b16, f32 = jnp.bfloat16, jnp.float32
    any_ = pl.BlockSpec(memory_space=pl.ANY)
    sem = pltpu.SemaphoreType.DMA
    return pl.pallas_call(
        kernel,
        out_shape=(
            jax.ShapeDtypeStruct((T, G * HD), b16),
            jax.ShapeDtypeStruct((T, HD), b16),
            jax.ShapeDtypeStruct((T, HD), b16),
            jax.ShapeDtypeStruct((RW, HD), f32),
        ),
        in_specs=[any_] * 5 + [pl.BlockSpec(memory_space=pltpu.SMEM), any_],
        out_specs=(any_,) * 4,
        scratch_shapes=[
            pltpu.VMEM((G, T, HD), b16),
            pltpu.VMEM((G, T, HD), b16),
            pltpu.VMEM((G, T, HD), b16),
            pltpu.VMEM((G, T), f32),
            pltpu.VMEM((6, T, HD), b16),
            pltpu.VMEM((6, T, HD), b16),
            pltpu.VMEM((24, T), f32),
            pltpu.VMEM((NB, BL, T), f32),
            pltpu.VMEM((5, G, T, T), f32),
            pltpu.VMEM((5, T, T), f32),
            pltpu.VMEM((5, T, HD), f32),
            pltpu.VMEM((5, T, HD), f32),
            pltpu.VMEM((G, T, HD), b16),
            pltpu.VMEM((2, HR, T), b16),
            pltpu.VMEM((4, 2, HR, T), b16),
            pltpu.VMEM((2, T, HD), b16),
            pltpu.VMEM((2, T, HD), b16),
            pltpu.VMEM((2, T, HD), b16),
            pltpu.VMEM((2, T, HD), b16),
            pltpu.VMEM((2, T, HD), b16),
            pltpu.VMEM((2, T, HD), b16),
            pltpu.VMEM((2, T, HD), b16),
            pltpu.VMEM((2, T, HD), b16),
            pltpu.VMEM((2, T, HD), b16),
            pltpu.VMEM((T, HD), b16),
            pltpu.VMEM((NZ, NY, RW, HD), b16),
            pltpu.VMEM((NZ, NY, RW, HD), b16),
            pltpu.VMEM((NY, NZ, RW, HD), b16),
            pltpu.VMEM((NY, RW, HD), b16),
            pltpu.VMEM((NZ, RW, HD), b16),
            pltpu.VMEM((NZ, RW, HD), b16),
            pltpu.VMEM((NY, RW, HD), b16),
            pltpu.VMEM((RW, HD), f32),
            sem((21,)),
            sem((32,)),
            sem((6,)),
            sem((6,)),
            sem((4, 2)),
            sem((2,)),
            sem((4,)),
            sem,
            sem((NZ,)),
            sem((NY,)),
            sem((NZ,)),
            sem((NY,)),
            sem((10,)),
        ],
        compiler_params=pltpu.CompilerParams(
            collective_id=0, has_side_effects=True, vmem_limit_bytes=60 * 1024 * 1024
        ),
        name="step",
    )(queries, keys, values, log_sums, out_grad, chosen, inputs)


def solution(mesh):
    return jax.shard_map(
        shards,
        mesh=mesh,
        in_specs=(
            P("kv", "tp"),
            P("kv", "tp"),
            P("kv", "tp"),
            P("tp", "kv"),
            P("kv", "tp"),
            P("kv", "tp", None),
            P("kv", "tp"),
        ),
        out_specs=(P("kv", "tp"), P("kv", "tp"), P("kv", "tp"), P("kv", "tp")),
        check_vma=False,
    )
```

time: 255 us -> 62.3 us (0.24)
  the two profiles are of different devices: /device:TPU:6 before, /device:TPU:1 now
where the time goes in v1:
time: 62.3 us; the launch traced here: 61.1 us
  Pallas kernels  56.4 us (91%)
  local copies, waits for them, and re-layouts  3.96 us (6%)
  between operations  0.65 us (1%)
    pallas_call x1, Pallas kernels, shards(): pl.pallas_call(kernel, out_shape=(jax.ShapeDtypeStruct((T, G * HD), b16),...  56.4 us
    unnamed x10, local copies, waits for them, and re-layouts  3.96 us

profile of v1, /device:TPU:1, one launch (start us, length us, event | category | flops | bytes accessed | tf_op | source)
XLA Modules:
  0.0 61.1 jit_solution(3574742876580714391)
XLA Ops:
  0.6 56.4 %step.1 = (bf16[256,768]{1,0:T(8,128)(2,1)}, bf16[256,128]{1,0:T(8,128)(2,1)}, bf16[256,128]{1,0:T(8,128)(2,1)}, f32[16,128]{1,0:T(8,128)}) custom-call(bf16[256,768]{1,0:T(8,128)(2,1)} %q_hbm.1, bf16[256,128]{1,0:T(8,128)(2,1)} %k_hbm.1, bf16[256,128]{1,0:T(8,128)(2,1)} %v_hbm.1, f32[6,256]{1,0:T(8,128)} %lse_hbm.1, bf16[256,768]{1,0:T(8,128)(2,1)} %do_hbm.1, ...), custom_call_target="tpu_custom_call" | custom-call | tf_op jit(solution)/shard_map/step/pallas_call | solution.py:356
  57.1 0.0 copy-start.1
  57.1 1.8 %copy.15 = bf16[256,768]{1,0:T(8,128)(2,1)} copy(bf16[256,768]{1,0:T(8,128)(2,1)} %get-tuple-element.8) | data formatting | bytes 786432
  58.9 0.0 copy-done.1
  58.9 0.0 copy-start
  58.9 0.6 %copy.16 = bf16[256,128]{1,0:T(8,128)(2,1)} copy(bf16[256,128]{1,0:T(8,128)(2,1)S(1)} %copy-done.1) | data formatting | bytes 131072
  59.5 0.2 copy-done
  59.8 0.0 copy-start.2
  59.8 0.6 %copy.17 = bf16[256,128]{1,0:T(8,128)(2,1)} copy(bf16[256,128]{1,0:T(8,128)(2,1)S(1)} %copy-done) | data formatting | bytes 131072
  60.4 0.1 copy-done.2
  60.5 0.6 copy.18
Async XLA Ops:
  57.1 1.8 %copy-start.1 = (bf16[256,128]{1,0:T(8,128)(2,1)S(1)}, bf16[256,128]{1,0:T(8,128)(2,1)}, u32[]{:S(2)}) copy-start(bf16[256,128]{1,0:T(8,128)(2,1)} %get-tuple-element.9) | copy-start | bytes 196612
  58.9 0.9 %copy-start = (bf16[256,128]{1,0:T(8,128)(2,1)S(1)}, bf16[256,128]{1,0:T(8,128)(2,1)}, u32[]{:S(2)}) copy-start(bf16[256,128]{1,0:T(8,128)(2,1)} %get-tuple-element.10) | copy-start | bytes 196612
  59.8 0.7 %copy-start.2 = (f32[16,128]{1,0:T(8,128)S(1)}, f32[16,128]{1,0:T(8,128)}, u32[]{:S(2)}) copy-start(f32[16,128]{1,0:T(8,128)} %get-tuple-element.11) | copy-start | bytes 24580

commit v2 on v1

v2 whole, which is shorter than its diff:
```python
import functools

import jax
import jax.numpy as jnp
from jax import lax
from jax.experimental import pallas as pl
from jax.experimental.pallas import tpu as pltpu
from jax.sharding import PartitionSpec as P

MESH = pl.DeviceIdType.MESH
LOG2E = 1.4426950408889634
MASKED = -1e30

NX, NY, NZ = 4, 8, 12
NCHIP = NY * NZ
T = 256
HD = 128
G = 6
BL = 64
NB = 4
SELS = 8
CPX = NCHIP // NX
RW = 16
HR = CPX * RW

NN = (((1,), (0,)), ((), ()))
NT = (((1,), (1,)), ((), ()))
TN = (((0,), (0,)), ((), ()))


def mm(a, b, dims):
    return lax.dot_general(a, b, dims, preferred_element_type=jnp.float32)


def kernel(
    q_hbm, k_hbm, v_hbm, lse_hbm, do_hbm, ch_hbm, in_hbm,
    dq_ref, dk_ref, dv_ref, dw_ref,
    ch_ref, q6, do6, in6, lse, kbuf, vbuf, hitb, ownb, pst, plow, dpst, dvacc, dkacc,
    hs, ing, sxv, rxv, sretv, rretv, sxk, rxk, sretk, rretk, vg,
    wpart, r1z, r1y, s1z, s1y, r2z, r2y,
    lsem, ssem, k_rs, v_rs, in_rs, x_rs, ret_rs, vg_rs, z_rs, y_rs, zs_s, ys_s, zk, yk,
):
    kv = lax.axis_index("kv")
    x = lax.axis_index("tp")
    p = kv // 2
    c = kv % 2
    z = p // NY
    y = p % NY
    o = 1 - c

    def wrapped(i, n):
        i = jnp.where(i >= n, i - n, i)
        return jnp.where(i < 0, i + n, i)

    def chip(step):
        return wrapped(p + step, NCHIP)

    def at(chip_id, core):
        return (chip_id * 2 + core, x)

    partner = at(p, o)
    nxt, prv, prv2, nxt2 = (at(chip(s), c) for s in (1, -1, -2, 2))
    xr, xl = wrapped(x + 1, NX), wrapped(x - 1, NX)

    def z_at(d):
        return wrapped(z + d, NZ)

    def y_at(d):
        return wrapped(y + d, NY)

    def z_dev(d):
        return at(z_at(d) * NY + y, c)

    def y_dev(d):
        return at(z * NY + y_at(d), c)

    loads = []

    def load(src, dst, n):
        copy = pltpu.make_async_copy(src, dst, lsem.at[n])
        copy.start()
        return copy

    ld_k = load(k_hbm, kbuf.at[4 + c], 0)
    ld_c = load(ch_hbm, ch_ref, 21)

    barrier = pltpu.get_barrier_semaphore()
    peers = [partner, nxt, nxt2, prv, prv2]
    peers += [(p * 2 + d, xx) for xx in (xr, xl) for d in (0, 1)]
    peers += [z_dev(1), z_dev(-1), y_dev(1), y_dev(-1)]
    for peer in peers:
        pl.semaphore_signal(barrier, inc=1, device_id=peer, device_id_type=MESH)

    def tell(k):
        for sem, dev, top in ((zk, z_dev, 3), (yk, y_dev, 2)):
            if k < top:
                for d in (1 << k, -(1 << k)):
                    pl.semaphore_signal(sem.at[k], inc=1, device_id=dev(d), device_id_type=MESH)

    def told(k):
        for sem, top in ((zk, 3), (yk, 2)):
            if k < top:
                with jax.named_scope(f"told{k}"):
                    pl.semaphore_wait(sem.at[k], 2)

    sends = []

    def send(src, dst, recv, device):
        n = len(sends)
        copy = pltpu.make_async_remote_copy(
            src_ref=src, dst_ref=dst, send_sem=ssem.at[n], recv_sem=recv,
            device_id=device, device_id_type=MESH,
        )
        copy.start()
        sends.append(copy)
        return copy

    waits = []

    def arrived(dst, recv):
        waits.append(0)
        with jax.named_scope(f'w{len(waits)}'):
            pltpu.make_async_copy(dst, dst, recv).wait()

    def kv_send(buf, rs, slot, device):
        send(buf.at[slot], buf.at[slot], rs.at[slot], device)

    def kv_send_to(buf, rs, src_slot, dst_slot, device):
        send(buf.at[src_slot], buf.at[dst_slot], rs.at[dst_slot], device)

    def half_of(slot, i):
        return kbuf.at[slot, pl.ds(i * (T // 2), T // 2)]

    def k_send(src_slot, dst_slot, i, device):
        send(half_of(src_slot, i), half_of(dst_slot, i), k_rs.at[dst_slot, i], device)

    def k_arrived(slot, i):
        arrived(half_of(slot, i), k_rs.at[slot, i])

    ld_k.wait()
    with jax.named_scope("w_barrier"):
        pl.semaphore_wait(barrier, len(peers))

    for i in (0, 1):
        k_send(4 + c, 2 + c, i, nxt)
    for i in (0, 1):
        k_send(4 + c, 4 + c, i, partner)
    ld_v = load(v_hbm, vbuf.at[4 + c], 8)
    ld_i = [load(in_hbm.at[:, pl.ds(HD * h, HD)], in6.at[h], 9 + h) for h in range(G)]
    ld_q = [load(q_hbm.at[:, pl.ds(HD * h, HD)], q6.at[h], 1 + h) for h in range(G)]
    ld_l = load(lse_hbm, lse, 7)
    ld_d = [load(do_hbm.at[:, pl.ds(HD * h, HD)], do6.at[h], 15 + h) for h in range(G)]
    ld_v.wait()
    kv_send_to(vbuf, v_rs, 4 + c, 2 + c, nxt)
    kv_send(vbuf, v_rs, 4 + c, partner)

    for j in range(G):
        ld_i[j].wait()
        xt = in6[j].T
        for m in range(4):
            for d in range(2):
                r0 = (4 * j + m) * RW
                hs[d, r0 : r0 + RW, :] = xt[32 * m + 16 * d : 32 * m + 16 * d + 16, :]

    send(hs.at[o], ing.at[0, c], in_rs.at[0, c], partner)
    def inputs_out(side_of_core):
        side = jnp.where(side_of_core == 0, xr, xl)
        rel = jnp.where(side_of_core == 0, 3, 1)
        for d in (0, 1):
            send(hs.at[d], ing.at[rel, c], in_rs.at[rel, c], (p * 2 + d, side))

    inputs_out(c)

    ld_c.wait()
    base = (p - 2) * 4 * 2 + 4 * c
    own0 = kv * NB
    wid = lax.broadcasted_iota(jnp.int32, (24, T), 0)
    lane = lax.broadcasted_iota(jnp.int32, (24, T), 1)
    hit = jnp.zeros((24, T), jnp.float32)
    for b in range(NB):
        in_b = (lane // BL) == b
        for k in range(SELS):
            named = ch_ref[b, 0, k]
            slot = jnp.where(named < own0 + b, named - base, -1)
            hit = jnp.where(in_b & (wid == slot), 1.0, hit)
    hitb[...] = jnp.where(hit > 0.5, 0.0, MASKED)
    krow = lax.broadcasted_iota(jnp.int32, (BL, T), 0)
    qlane = lax.broadcasted_iota(jnp.int32, (BL, T), 1)
    for j in range(NB):
        here = (qlane // BL) == j
        causal = here & (krow <= qlane - BL * j)
        ownb[j] = jnp.where(causal, 0.0, jnp.where(here, MASKED, hitb[16 + j : 17 + j, :]))

    for copy in ld_q:
        copy.wait()
    ld_l.wait()
    for copy in ld_d:
        copy.wait()

    lse[...] = lse[...] * LOG2E
    factor = HD ** (-0.5) * LOG2E

    def value_terms(s):
        with jax.named_scope(f"value_terms{s}"):
            keys = kbuf[s + c]
            for h in range(G):
                scores = mm(keys, q6[h], NT)
                row = lse[h : h + 1, :]
                for j in range(NB):
                    part = scores[BL * j : BL * j + BL, :] * factor
                    if s == 4:
                        shift = ownb[j] - row
                    else:
                        shift = hitb[4 * s + j : 4 * s + j + 1, :] - row
                    part = jnp.exp2(part + shift)
                    pst[s, h, BL * j : BL * j + BL, :] = part
                    plow[s, BL * j : BL * j + BL, T * h : T * h + T] = part.astype(jnp.bfloat16)
            half = G // 2
            dvacc[s] = mm(
                plow[s, :, : T * half], do6[:half].reshape(T * half, HD), NN
            ) + mm(plow[s, :, T * half :], do6[half:].reshape(T * half, HD), NN)

    tell(0)
    value_terms(4)
    for i in (0, 1):
        k_arrived(2 + c, i)
        k_send(2 + c, c, i, nxt)
        k_send(2 + c, 2 + c, i, partner)
    value_terms(2)
    arrived(vbuf.at[2 + c], v_rs.at[2 + c])
    kv_send_to(vbuf, v_rs, 2 + c, c, nxt)
    kv_send(vbuf, v_rs, 2 + c, partner)
    for slot in (2 + o, 4 + o):
        for i in (0, 1):
            k_arrived(slot, i)
    inputs_out(o)
    value_terms(3)
    for i in (0, 1):
        k_arrived(c, i)
        k_send(c, c, i, partner)
    value_terms(0)
    for i in (0, 1):
        k_arrived(o, i)
    value_terms(1)

    sxv[0] = dvacc[1].astype(jnp.bfloat16)
    sxv[1] = dvacc[3].astype(jnp.bfloat16)
    send(sxv, rxv, x_rs.at[0], partner)
    arrived(ing.at[3, 0], in_rs.at[3, 0])
    send(ing.at[3, 0], ing.at[2, 0], in_rs.at[2, 0], (kv, xr))
    arrived(ing.at[1, 1], in_rs.at[1, 1])
    send(ing.at[1, 1], ing.at[2, 1], in_rs.at[2, 1], (kv, xl))
    told(0)
    tell(1)

    def score_terms(h):
        with jax.named_scope(f"score_terms{h}"):
            delta = jnp.zeros((1, T), jnp.float32)
            for s in range(5):
                dp = mm(vbuf[s + c], do6[h], NT)
                dpst[h % 2, s] = dp
                delta = delta + jnp.sum(pst[s, h] * dp, axis=0, keepdims=True)
            dqt = jnp.zeros((HD, T), jnp.float32)
            for s in range(5):
                ds = (pst[s, h] * (dpst[h % 2, s] - delta)).astype(jnp.bfloat16)
                if h == 0:
                    dkacc[s] = mm(ds, q6[h], NN)
                else:
                    dkacc[s] += mm(ds, q6[h], NN)
                dqt = dqt + mm(kbuf[s + c], ds, TN)
            dq_ref[:, HD * h : HD * h + HD] = (dqt * HD ** (-0.5)).T.astype(jnp.bfloat16)

    arrived(vbuf.at[c], v_rs.at[c])
    kv_send(vbuf, v_rs, c, partner)

    arrived(rxv, x_rs.at[0])
    for k in range(2):
        dvacc[2 * k + 2 * o] += rxv[k].astype(jnp.float32)
    sretv[0] = dvacc[0].astype(jnp.bfloat16)
    sretv[1] = dvacc[2].astype(jnp.bfloat16)
    send(sretv.at[0], rretv.at[0], ret_rs.at[0], prv2)
    send(sretv.at[1], rretv.at[1], ret_rs.at[1], prv)

    for slot in (2 + o, 4 + o, o):
        arrived(vbuf.at[slot], v_rs.at[slot])
    score_terms(0)
    score_terms(1)
    told(1)
    tell(2)
    score_terms(2)
    score_terms(3)

    for k in range(2):
        arrived(rretv.at[k], ret_rs.at[k])
    total = dvacc[4] + rretv[0].astype(jnp.float32) + rretv[1].astype(jnp.float32)
    vg[c] = total.astype(jnp.bfloat16)
    send(vg.at[c], vg.at[c], vg_rs, partner)
    dv_ref[...] = vg[c]
    score_terms(4)
    told(2)

    arrived(ing.at[0, o], in_rs.at[0, o])
    arrived(ing.at[3, 1], in_rs.at[3, 1])
    arrived(ing.at[1, 0], in_rs.at[1, 0])
    for d in (0, 1):
        arrived(ing.at[2, d], in_rs.at[2, d])
    arrived(vg.at[o], vg_rs)

    for rel in range(4):
        if rel == 0:
            rows = mm(hs[c], vg[c], NN) + mm(ing[0, o], vg[o], NN)
        else:
            rows = mm(ing[rel, 0], vg[0], NN) + mm(ing[rel, 1], vg[1], NN)
        first = wrapped(x + rel, NX) * (CPX // NY)
        tiles = rows.astype(jnp.bfloat16).reshape(CPX, RW, HD)
        for a in range(CPX // NY):
            wpart[first + a] = tiles[a * NY : (a + 1) * NY]

    def fan(n, src, dst, recv, sem, device, start=True):
        copies = []
        for d in range(1, n):
            copy = pltpu.make_async_remote_copy(
                src_ref=src(d), dst_ref=dst.at[d], send_sem=sem.at[d], recv_sem=recv.at[d],
                device_id=device(d), device_id_type=MESH,
            )
            if start:
                copy.start()
            copies.append(copy)
        return copies

    def total_of(n, own, got, recv):
        acc = own.astype(jnp.float32)
        for d in range(1, n):
            arrived(got.at[d], recv.at[d])
            acc = acc + got[d].astype(jnp.float32)
        return acc

    def first_z(start):
        return fan(NZ, lambda d: wpart.at[z_at(d)], r1z, z_rs, zs_s, z_dev, start)

    def first_y(start):
        return fan(NY, lambda d: wpart.at[:, y_at(d)], r1y, y_rs, ys_s, y_dev, start)

    @pl.when(c == 1)
    def _():
        first_z(True)

    @pl.when(c == 0)
    def _():
        first_y(True)

    score_terms(5)
    sxk[0] = dkacc[1].astype(jnp.bfloat16)
    sxk[1] = dkacc[3].astype(jnp.bfloat16)
    send(sxk, rxk, x_rs.at[1], partner)
    arrived(rxk, x_rs.at[1])
    for k in range(2):
        dkacc[2 * k + 2 * o] += rxk[k].astype(jnp.float32)
    sretk[0] = dkacc[0].astype(jnp.bfloat16)
    send(sretk.at[0], rretk.at[0], ret_rs.at[2], prv)

    def second_y(start):
        return fan(NY, lambda d: s1z.at[y_at(d)], r2y, y_rs, ys_s, y_dev, start)

    def second_z(start):
        return fan(NZ, lambda d: s1y.at[z_at(d)], r2z, z_rs, zs_s, z_dev, start)

    @pl.when(c == 1)
    def _():
        s1z[...] = total_of(NZ, wpart[z], r1z, z_rs).astype(jnp.bfloat16)
        second_y(True)

    @pl.when(c == 0)
    def _():
        s1y[...] = total_of(NY, wpart[:, y], r1y, y_rs).astype(jnp.bfloat16)
        second_z(True)

    arrived(rretk.at[0], ret_rs.at[2])
    sretk[1] = (dkacc[2] + rretk[0].astype(jnp.float32)).astype(jnp.bfloat16)
    send(sretk.at[1], rretk.at[1], ret_rs.at[3], prv)

    @pl.when(c == 1)
    def _():
        dw_ref[...] = total_of(NY, s1z[y], r2y, y_rs)
        for copy in first_z(False) + second_y(False):
            copy.wait_send()

    @pl.when(c == 0)
    def _():
        dw_ref[...] = total_of(NZ, s1y[z], r2z, z_rs)
        for copy in first_y(False) + second_z(False):
            copy.wait_send()

    arrived(rretk.at[1], ret_rs.at[3])
    key_total = dkacc[4] + rretk[1].astype(jnp.float32)
    dk_ref[...] = (key_total * HD ** (-0.5)).astype(jnp.bfloat16)
    for copy in sends:
        copy.wait_send()


def put_out(*refs):
    n = len(refs) // 2
    sems = refs[-1]
    copies = [pltpu.make_async_copy(refs[i], refs[n + i], sems.at[i]) for i in range(n)]
    for copy in copies:
        copy.start()
    for copy in copies:
        copy.wait()


def shards(queries, keys, values, log_sums, out_grad, chosen, inputs):
    b16, f32 = jnp.bfloat16, jnp.float32
    any_ = pl.BlockSpec(memory_space=pl.ANY)
    sem = pltpu.SemaphoreType.DMA
    results = pl.pallas_call(
        kernel,
        out_shape=(
            pltpu.VMEM((T, G * HD), b16),
            pltpu.VMEM((T, HD), b16),
            pltpu.VMEM((T, HD), b16),
            pltpu.VMEM((RW, HD), f32),
        ),
        in_specs=[any_] * 7,
        out_specs=(pl.BlockSpec(memory_space=pltpu.VMEM),) * 4,
        scratch_shapes=[
            pltpu.SMEM((NB, 1, SELS), jnp.int32),
            pltpu.VMEM((G, T, HD), b16),
            pltpu.VMEM((G, T, HD), b16),
            pltpu.VMEM((G, T, HD), b16),
            pltpu.VMEM((G, T), f32),
            pltpu.VMEM((6, T, HD), b16),
            pltpu.VMEM((6, T, HD), b16),
            pltpu.VMEM((24, T), f32),
            pltpu.VMEM((NB, BL, T), f32),
            pltpu.VMEM((5, G, T, T), f32),
            pltpu.VMEM((5, T, G * T), b16),
            pltpu.VMEM((2, 5, T, T), f32),
            pltpu.VMEM((5, T, HD), f32),
            pltpu.VMEM((5, T, HD), f32),
            pltpu.VMEM((2, HR, T), b16),
            pltpu.VMEM((4, 2, HR, T), b16),
            pltpu.VMEM((2, T, HD), b16),
            pltpu.VMEM((2, T, HD), b16),
            pltpu.VMEM((2, T, HD), b16),
            pltpu.VMEM((2, T, HD), b16),
            pltpu.VMEM((2, T, HD), b16),
            pltpu.VMEM((2, T, HD), b16),
            pltpu.VMEM((2, T, HD), b16),
            pltpu.VMEM((2, T, HD), b16),
            pltpu.VMEM((2, T, HD), b16),
            pltpu.VMEM((NZ, NY, RW, HD), b16),
            pltpu.VMEM((NZ, NY, RW, HD), b16),
            pltpu.VMEM((NY, NZ, RW, HD), b16),
            pltpu.VMEM((NY, RW, HD), b16),
            pltpu.VMEM((NZ, RW, HD), b16),
            pltpu.VMEM((NZ, RW, HD), b16),
            pltpu.VMEM((NY, RW, HD), b16),
            sem((22,)),
            sem((48,)),
            sem((6, 2)),
            sem((6,)),
            sem((4, 2)),
            sem((2,)),
            sem((4,)),
            sem,
            sem((NZ,)),
            sem((NY,)),
            sem((NZ,)),
            sem((NY,)),
            pltpu.SemaphoreType.REGULAR((3,)),
            pltpu.SemaphoreType.REGULAR((2,)),
        ],
        compiler_params=pltpu.CompilerParams(
            collective_id=0, has_side_effects=True, vmem_limit_bytes=66450000
        ),
        name="step",
    )(queries, keys, values, log_sums, out_grad, chosen, inputs)
    return pl.pallas_call(
        put_out,
        out_shape=tuple(jax.ShapeDtypeStruct(r.shape, r.dtype) for r in results),
        in_specs=[pl.BlockSpec(memory_space=pltpu.VMEM)] * 4,
        out_specs=(any_,) * 4,
        scratch_shapes=[sem((4,))],
        compiler_params=pltpu.CompilerParams(vmem_limit_bytes=1 << 20),
        name="put_out",
    )(*results)


def solution(mesh):
    return jax.shard_map(
        shards,
        mesh=mesh,
        in_specs=(
            P("kv", "tp"),
            P("kv", "tp"),
            P("kv", "tp"),
            P("tp", "kv"),
            P("kv", "tp"),
            P("kv", "tp", None),
            P("kv", "tp"),
        ),
        out_specs=(P("kv", "tp"), P("kv", "tp"), P("kv", "tp"), P("kv", "tp")),
        check_vma=False,
    )
```

time: 62.3 us -> 53.8 us (0.86); the launches traced: 61.1 us -> 53.6 us
  local copies, waits for them, and re-layouts: 3.96 us -> 0 us
  Pallas kernels: 56.4 us -> 52.9 us
    unnamed x10 -> x0, local copies, waits for them, and re-layouts: 3.96 us -> none
    pallas_call x1 -> x2, Pallas kernels: 56.4 us -> 52.9 us  [the longest x1 52.1 us: shards(): pl.pallas_call(kernel, out_shape=(pltpu.VMEM((T, G * HD), b16), pltpu.VME...]
where the time goes in v2:
time: 53.8 us; the launch traced here: 53.6 us
  Pallas kernels  52.9 us (98%)
  between operations  0.64 us (1%)
    pallas_call x1, Pallas kernels, shards(): pl.pallas_call(kernel, out_shape=(pltpu.VMEM((T, G * HD), b16), pltpu.VME...  52.1 us

profile of v2, /device:TPU:1, one launch (start us, length us, event | category | flops | bytes accessed | tf_op | source)
XLA Modules:
  0.0 53.6 jit_solution(6549390086882307455)
XLA Ops:
  0.6 52.1 %step.1 = (bf16[256,768]{1,0:T(8,128)(2,1)S(1)}, bf16[256,128]{1,0:T(8,128)(2,1)S(1)}, bf16[256,128]{1,0:T(8,128)(2,1)S(1)}, f32[16,128]{1,0:T(8,128)S(1)}) custom-call(bf16[256,768]{1,0:T(8,128)(2,1)} %q_hbm.1, bf16[256,128]{1,0:T(8,128)(2,1)} %k_hbm.1, bf16[256,128]{1,0:T(8,128)(2,1)} %v_hbm.1, f32[6,256]{1,0:T(8,128)} %lse_hbm.1, ...), custom_call_target="tpu_custom_call" | custom-call | tf_op jit(solution)/shard_map/step/pallas_call | solution.py:415
  52.8 0.8 %put_out.1 = (bf16[256,768]{1,0:T(8,128)(2,1)}, bf16[256,128]{1,0:T(8,128)(2,1)}, bf16[256,128]{1,0:T(8,128)(2,1)}, f32[16,128]{1,0:T(8,128)}) custom-call(bf16[256,768]{1,0:T(8,128)(2,1)S(1)} %get-tuple-element.8.refs_0_, bf16[256,128]{1,0:T(8,128)(2,1)S(1)} %get-tuple-element.9.refs_1_, bf16[256,128]{1,0:T(8,128)(2,1)S(1)} %get-tuple-element.10.refs_2_, ...), custom_call_target="tpu_custom_call" | custom-call | tf_op jit(solution)/shard_map/put_out/pallas_call | solution.py:478
